TPU v7x, 512 devices: a 4x2x32 block of a 4x8x32 slice. The times are simulated.
512 devices in a mesh: grp: 2 (over y), kv: 64 (over z, core), tp: 4 (over x).
Axes of the slice: x: 4, y: 2, z: 32, core: 2. Of those that a mesh axis runs over, the one named last changes fastest.
The devices are a block of a 4x8x32 slice.
Arguments:
- tokens: bfloat16 [65536, 2048], P(('grp', 'kv')), parts along dimension 0, may hold values from -72 to 72
- w_query: bfloat16 [2048, 1024], P(None, 'tp'), may hold values from -0.125 to 0.125
- w_key: bfloat16 [2048, 256], P(None, 'tp'), may hold values from -0.125 to 0.125
- w_value: bfloat16 [2048, 256], P(None, 'tp'), may hold values from -0.125 to 0.125
- w_out: bfloat16 [1024, 2048], P('tp'), may hold values from -0.1875 to 0.1875
- selection: int32 [4, 1024, 32], P('tp', ('grp', 'kv')), parts along dimension 1, may hold values from -1 to 511, as said below
Outputs:
- attended_out: bfloat16 [65536, 2048], P(('grp', 'kv', 'tp')), parts along dimension 0
There are 2 independent parts, one for each index of `grp`. A program takes and returns all parts, laid end to end along the dimension named above; an argument that names none is the same for every part. Nothing has to cross between parts.
Inputs may be any that keep to these rules, and one draw needn't show every extreme that they name: `selection`: entry 0 is the query block's own index; the others are distinct indices of earlier blocks, then -1 for unused entries. For one key head, the query blocks of one device's range together choose at most 2 distinct blocks of any other device's range, and some device reaches 2 in every draw.
All inputs are finite; a program needn't handle non-finite values.
Results may differ from a plain program's by a relative error of at most 0.028.
The roundings to bfloat16 on the way count: a program that leaves them out, or rounds other values in their place, can miss the bound.
Values may be sent and summed in bfloat16 or wider, within the bound.
No kernel may reach another device: no remote copies, remote signals or barrier semaphores. Data moves between devices by JAX's collectives and lax.ppermute only.
A program may use at most 128 MiB of HBM per device.

v0:
```python
import jax
import jax.numpy as jnp
from jax import lax
from jax.sharding import PartitionSpec as P

HEAD_DIM = 64
BLOCK = 64
TOPK = 32


ROPE_BASE = 500000.0


def cut_along(shard, dim, peers):
    lengths = shard.shape
    tiles = shard.reshape(*lengths[:dim], peers, lengths[dim] // peers, *lengths[dim + 1 :])
    return jnp.moveaxis(tiles, dim, 0)


def sum_at_owner(shard, axis, dim):
    tiles = cut_along(shard, dim, lax.axis_size(axis))
    arrived = lax.all_to_all(tiles, axis, split_axis=0, concat_axis=0, tiled=True)
    return arrived.astype(jnp.float32).sum(axis=0)


def rotate(head_rows, positions):
    half = head_rows.shape[-1] // 2
    freqs = ROPE_BASE ** (-jnp.arange(half, dtype=jnp.float32) / half)
    angles = positions[:, None, None] * freqs
    cosine = jnp.cos(angles)
    sine = jnp.sin(angles)
    first = head_rows[..., :half]
    second = head_rows[..., half:]
    return jnp.concatenate(
        [first * cosine - second * sine, second * cosine + first * sine], axis=-1
    )


def shards(tokens, w_query, w_key, w_value, w_out, selection):
    row_count = tokens.shape[0]
    local_heads = w_query.shape[1] // HEAD_DIM
    own_index = lax.axis_index("kv")
    positions_int = own_index * row_count + jnp.arange(row_count)
    positions = positions_int.astype(jnp.float32)
    queries = rotate(
        jnp.dot(tokens, w_query, preferred_element_type=jnp.float32).reshape(
            row_count, local_heads, HEAD_DIM
        ),
        positions,
    ).astype(jnp.bfloat16)
    key_local = rotate(
        jnp.dot(tokens, w_key, preferred_element_type=jnp.float32).reshape(row_count, 1, HEAD_DIM),
        positions,
    )[:, 0].astype(jnp.bfloat16)
    value_local = jnp.dot(tokens, w_value, preferred_element_type=jnp.float32).astype(jnp.bfloat16)
    key_value = jnp.concatenate([key_local, value_local], axis=-1)
    blocks_here = row_count // BLOCK
    chosen_ids = selection[0]
    key_table = lax.all_gather(key_value, "kv", axis=0, tiled=True).reshape(-1, BLOCK, 2 * HEAD_DIM)
    slot_ids = jnp.maximum(chosen_ids, 0)
    picked = key_table[slot_ids]
    picked_keys = picked[..., :HEAD_DIM].reshape(blocks_here, TOPK * BLOCK, HEAD_DIM)
    picked_values = picked[..., HEAD_DIM:].reshape(blocks_here, TOPK * BLOCK, HEAD_DIM)
    offsets = jnp.arange(BLOCK)
    key_pos = (chosen_ids[:, :, None] * BLOCK + offsets).reshape(blocks_here, TOPK * BLOCK)
    live_keys = jnp.repeat(chosen_ids >= 0, BLOCK, axis=1)
    query_pos = positions_int.reshape(blocks_here, BLOCK)
    query_rows = queries.reshape(blocks_here, BLOCK, local_heads, HEAD_DIM)
    scores = jnp.einsum(
        "qbhd,qkd->qhbk", query_rows, picked_keys, preferred_element_type=jnp.float32
    ) * HEAD_DIM ** (-0.5)
    allowed = live_keys[:, None, None, :] & (
        key_pos[:, None, None, :] <= query_pos[:, None, :, None]
    )
    scores = jnp.where(allowed, scores, -jnp.inf)
    top_score = jnp.max(scores, axis=-1, keepdims=True)
    expo = jnp.exp(scores - top_score)
    weights = (expo / jnp.sum(expo, axis=-1, keepdims=True)).astype(jnp.bfloat16)
    attended = jnp.einsum(
        "qhbk,qkd->qbhd", weights, picked_values, preferred_element_type=jnp.float32
    ).astype(jnp.bfloat16)
    attended = attended.reshape(row_count, local_heads * HEAD_DIM)
    summed = sum_at_owner(
        jnp.dot(attended, w_out, preferred_element_type=jnp.float32).astype(jnp.bfloat16), "tp", 0
    )
    return summed.astype(jnp.bfloat16)


def solution(mesh):
    placed = (
        P(("grp", "kv"), None),
        P(None, "tp"),
        P(None, "tp"),
        P(None, "tp"),
        P("tp", None),
        P("tp", ("grp", "kv"), None),
    )
    return jax.shard_map(
        shards, mesh=mesh, in_specs=placed, out_specs=P(("grp", "kv", "tp"), None), check_vma=False
    )
```

profile of v0, /device:TPU:33, one launch (start us, length us, event | category | flops | bytes accessed | tf_op | source)
XLA Modules:
  0.0 269.1 jit_solution(14196923973627354760)
XLA Ops:
  6.6 1.6 copy-done
  8.1 1.7 convolution_convert_fusion.1
  9.8 1.7 convolution_bitcast_fusion
  11.6 0.3 fusion.16
  11.9 0.7 pad_maximum_fusion.1
  12.9 0.1 and.16
  13.3 0.3 multiply_cosine_fusion
  13.6 2.0 fusion.27
  15.6 0.2 concatenate.18
  15.8 1.1 copy.12
  17.0 0.2 concatenate.19
  17.2 1.1 copy.13
  18.3 1.0 compare_and_fusion
  19.3 160.9 %all-gather.2.cloned.1.call-done = bf16[32768,128]{0,1:T(8,128)(2,1)} async-done(((bf16[512,128]{0,1:T(8,128)(2,1)}), bf16[32768,128]{0,1:T(8,128)(2,1)}) %all-gather.2.cloned.1.call-update) | async-done | bytes 8388624 | tf_op jit(solution)/shard_map/all_gather | solution.py:59
  180.2 11.9 %copy.9 = bf16[32768,128]{1,0:T(8,128)(2,1)} copy(bf16[32768,128]{0,1:T(8,128)(2,1)} %all-gather.2.cloned.1.call-done) | data formatting | bytes 16777216 | tf_op jit(solution)/shard_map/all_gather | solution.py:59
  192.1 6.4 %gather_fusion = bf16[256,64,128]{2,1,0:T(8,128)(2,1)} fusion(bf16[512,64,128]{2,1,0:T(8,128)(2,1)} %bitcast.53, s32[1024]{0:T(1024)S(1)} %pad_clamp_fusion), kind=kCustom, calls=%fused_computation | custom fusion | bytes 8389632 | tf_op jit(solution)/shard_map/gather | solution.py:61
  198.5 7.3 %fusion.25 = (bf16[8,32,64,64]{3,2,1,0:T(8,128)(2,1)}, bf16[8,32,64,64]{3,2,1,0:T(8,128)(2,1)}) fusion(bf16[8,32,64,128]{3,2,1,0:T(8,128)(2,1)} %bitcast.52), kind=kLoop, calls=%fused_computation.47 | loop fusion | bytes 8388608 | tf_op jit(solution)/shard_map/slice | solution.py:62
  205.8 10.6 %fusion.26 = (f32[8,4,64]{2,1,0:T(4,128)S(1)}, f32[8,4,64,2048]{3,2,1,0:T(8,128)}) fusion(pred[8,64,2048]{2,1,0:T(8,128)(4,1)S(1)} %compare_and_fusion, bf16[8,2048,64,1]{2,1,3,0:T(8,128)(2,1)} %bitcast.56, bf16[8,64,4,32]{3,1,2,0:T(8,128)(2,1)} %copy.13, bf16[8,64,4,32]{3,1,2,0:T(8,128)(2,1)} %copy.12), kind=kOutput, calls=%fused_computation.48 | convolution fusion | flops 554174464 | bytes 20193280 | tf_op jit(solution)/shard_map/sub | solution.py:77
  216.4 10.7 %fusion.9 = bf16[8,64,4,64]{1,3,2,0:T(8,128)(2,1)S(1)} fusion(bf16[8,2048,64,1]{2,1,3,0:T(8,128)(2,1)} %bitcast.55, f32[8,4,64,2048]{3,2,1,0:T(8,128)} %get-tuple-element.16, f32[8,4,64]{2,1,0:T(4,128)S(1)} %get-tuple-element.15), kind=kOutput, calls=%fused_computation.14 | convolution fusion | flops 545390592 | bytes 19144704 | tf_op jit(solution)/shard_map/qhbk,qkd->qbhd/dot_general | solution.py:79
  227.1 0.3 copy.14
  227.5 0.3 reshape.205
  227.8 2.0 convolution_convert_fusion
  229.8 29.6 %all_to_all.5 = bf16[4,128,2048]{2,1,0:T(8,128)(2,1)} all-to-all(bf16[4,128,2048]{2,1,0:T(8,128)(2,1)S(1)} %bitcast.54), channel_id=1, replica_groups=mesh['grp'=2,'kv'=64,'tp'=4] {'tp'}, dimensions={0} | all-to-all | bytes 4194304 | tf_op jit(solution)/shard_map/all_to_all | solution.py:22
  259.4 2.9 %reduce_sum.22 = bf16[128,2048]{1,0:T(8,128)(2,1)} reduce(bf16[4,128,2048]{2,1,0:T(8,128)(2,1)} %all_to_all.5, bf16[]{:T(256)} %constant.29.clone.1), dimensions={0}, to_apply=%region_2.3 | reduce | flops 786432 | bytes 2621442 | tf_op jit(solution)/shard_map/reduce_sum | solution.py:23
  (20 shorter events, 0.6 us)
Async XLA Ops:
  6.5 1.6 copy-start
  6.6 6.1 %copy-start.1 = (s32[1,8,32]{2,1,0:T(8,128)S(1)}, s32[1,8,32]{2,1,0:T(8,128)}, u32[]{:S(2)}) copy-start(s32[1,8,32]{2,1,0:T(8,128)} %param.11) | copy-start | bytes 3076
  6.6 173.6 %all-gather.2.cloned.1.call-start = ((), (), s32[]{:S(2)}) async-start(), calls=%async_computation.1 | async-start | bytes 8519680 | tf_op jit(solution)/shard_map/all_gather | solution.py:59
Sparse Core Ops, SparseCore 0:
  12.8 167.3 all-gather.1
where the time goes:
time: 270 us; the launch traced here: 269 us
  waiting for transfers between devices  161 us (60%)
  local copies, waits for them, and re-layouts  31 us (11%)
  blocking collectives  29.6 us (11%)
  matrix products  28.6 us (11%)
  between operations  13.6 us (5%)
  other arithmetic  5.32 us (2%)
    all_gather x1, waiting for transfers between devices, shards(): lax.all_gather(key_value, 'kv', axis=0, tiled=True)  161 us
    all_to_all x1, blocking collectives, sum_at_owner(): lax.all_to_all(tiles, axis, split_axis=0, concat_axis=0, tiled=True)  29.6 us
    all_gather x1, local copies, waits for them, and re-layouts, shards(): lax.all_gather(key_value, 'kv', axis=0, tiled=True)  11.9 us
    dot_general x1, matrix products, shards(): jnp.einsum('qhbk,qkd->qbhd', weights, picked_values, preferred_element_ty...  10.7 us
    sub x1, matrix products, shards(): expo = jnp.exp(scores - top_score)  10.6 us
    slice x1, local copies, waits for them, and re-layouts, shards(): picked[..., :HEAD_DIM].reshape(blocks_here, TOPK * BLOCK, HEAD_DIM)  7.28 us
    gather x1, local copies, waits for them, and re-layouts, shards(): picked = key_table[slot_ids]  6.41 us
  transfers between devices with their start and end apart: 1, of which 1 were waited for; matrix products, arithmetic and copies ran while one was open for 2% of the time, Pallas kernels for 0%

commit v1 on v0

v1 whole, which is shorter than its diff:
```python
import functools

import jax
import jax.numpy as jnp
from jax import lax
from jax.experimental import pallas as pl
from jax.experimental.pallas import tpu as pltpu
from jax.sharding import PartitionSpec as P

HEAD_DIM = 64
BLOCK = 64
ROPE_BASE = 500000.0
LANES = 2 * HEAD_DIM
HALF = HEAD_DIM // 2


def encode(x):
    mag = jnp.abs(x)
    live = mag >= 2.0**-126
    safe = jnp.where(live, mag, 1.0)
    exponent = jnp.floor(jnp.log2(safe))
    exponent = jnp.clip(exponent, -126.0, 127.0)
    half_exp = jnp.floor(exponent * 0.5)
    ratio = safe * jnp.exp2(-half_exp) * jnp.exp2(half_exp - exponent)
    code = (exponent + 126.0) * 128.0 + jnp.floor(ratio * 128.0 + 0.5)
    code = jnp.where(live, code, 0.0)
    return jnp.where(x < 0, -code, code).astype(jnp.int32).astype(jnp.int16)


def decode(code):
    signed = code.astype(jnp.int32).astype(jnp.float32)
    level = jnp.abs(signed) * (1.0 / 128.0)
    whole = jnp.floor(level)
    mag = (level - whole + 1.0) * jnp.exp2(whole - 127.0)
    return jnp.where(signed < 0, -mag, mag).astype(jnp.bfloat16)


def swap_halves(x, lane):
    return jnp.where(
        lane % HEAD_DIM < HALF,
        pltpu.roll(x, LANES - HALF, 1),
        pltpu.roll(x, HALF, 1),
    )


def project_body(tok_ref, wq_ref, wk_ref, wv_ref, cos_ref, sin_ref, code_ref, q_ref, wkv_ref):
    @pl.when(pl.program_id(0) == 0)
    def _():
        wkv_ref[:, :HEAD_DIM] = wk_ref[...]
        wkv_ref[:, HEAD_DIM:] = wv_ref[...]

    tok = tok_ref[...]
    rows = tok.shape[0]
    lane = lax.broadcasted_iota(jnp.int32, (rows, LANES), 1)
    cosine = cos_ref[...]
    sine = sin_ref[...]
    kv = jnp.dot(tok, wkv_ref[...], preferred_element_type=jnp.float32)
    is_key = lane < HEAD_DIM
    kv = jnp.where(is_key, kv * cosine + swap_halves(kv, lane) * sine, kv)
    code_ref[...] = encode(kv.astype(jnp.bfloat16).astype(jnp.float32))
    q_all = jnp.dot(tok, wq_ref[...], preferred_element_type=jnp.float32)
    heads = q_all.shape[1] // HEAD_DIM
    for pair in range(heads // 2):
        q = q_all[:, pair * LANES : (pair + 1) * LANES]
        q = q * cosine + swap_halves(q, lane) * sine
        q = q.astype(jnp.bfloat16).astype(jnp.float32) * HEAD_DIM**-0.5
        for odd in range(2):
            one = pltpu.roll(q, HEAD_DIM, 1) if odd else q
            one = jnp.where(is_key, one, 0.0).astype(jnp.bfloat16)
            for b in range(rows // BLOCK):
                at = (2 * pair + odd) * BLOCK
                q_ref[b, at : at + BLOCK, :] = one[b * BLOCK : (b + 1) * BLOCK]


def project(tokens, w_query, w_key, w_value, cosine, sine):
    rows, width = tokens.shape
    qcols = w_query.shape[1]
    heads = qcols // HEAD_DIM
    tile = 128
    return pl.pallas_call(
        project_body,
        grid=(rows // tile,),
        in_specs=[
            pl.BlockSpec((tile, width), lambda i: (i, 0)),
            pl.BlockSpec((width, qcols), lambda i: (0, 0)),
            pl.BlockSpec((width, HEAD_DIM), lambda i: (0, 0)),
            pl.BlockSpec((width, HEAD_DIM), lambda i: (0, 0)),
            pl.BlockSpec((tile, LANES), lambda i: (i, 0)),
            pl.BlockSpec((tile, LANES), lambda i: (i, 0)),
        ],
        out_specs=[
            pl.BlockSpec((tile, LANES), lambda i: (i, 0)),
            pl.BlockSpec((tile // BLOCK, heads * BLOCK, LANES), lambda i: (i, 0, 0)),
        ],
        out_shape=[
            jax.ShapeDtypeStruct((rows, LANES), jnp.int16),
            jax.ShapeDtypeStruct((rows // BLOCK, heads * BLOCK, LANES), jnp.bfloat16),
        ],
        scratch_shapes=[pltpu.VMEM((width, LANES), jnp.bfloat16)],
        compiler_params=pltpu.CompilerParams(dimension_semantics=("arbitrary",)),
        name="project",
    )(tokens, w_query, w_key, w_value, cosine, sine)


def attend_body(sel_ref, q_ref, bias_ref, table_ref, out_ref, kv_ref, s_ref, p_ref, *, topk):
    b = pl.program_id(0)
    for t in range(topk):
        at = pl.multiple_of(jnp.maximum(sel_ref[b, t], 0) * BLOCK, BLOCK)
        kv_ref[t * BLOCK : (t + 1) * BLOCK, :] = decode(table_ref[pl.ds(at, BLOCK), :])
    q = q_ref[0]
    rows = q.shape[0]
    s_ref[...] = lax.dot_general(
        q, kv_ref[...], (((1,), (1,)), ((), ())), preferred_element_type=jnp.float32
    )
    chunk = 32
    bias = bias_ref[0]
    sums = []
    for r in range(0, rows, chunk):
        s = s_ref[r : r + chunk, :] + bias
        row = lax.broadcasted_iota(jnp.int32, (chunk, LANES), 0) + r % BLOCK
        col = lax.broadcasted_iota(jnp.int32, (chunk, LANES), 1)
        first = jnp.where((col < BLOCK) & (col > row), -jnp.inf, s[:, :LANES])
        s = jnp.concatenate([first, s[:, LANES:]], axis=1)
        e = jnp.exp(s - jnp.max(s, axis=1, keepdims=True))
        sums.append(jnp.sum(e, axis=1, keepdims=True))
        p_ref[r : r + chunk, :] = e.astype(jnp.bfloat16)
    o = jnp.dot(p_ref[...], kv_ref[...], preferred_element_type=jnp.float32)
    o = o / jnp.concatenate(sums, axis=0)
    lane = lax.broadcasted_iota(jnp.int32, (BLOCK, LANES), 1)
    for pair in range(rows // BLOCK // 2):
        even = o[2 * pair * BLOCK : (2 * pair + 1) * BLOCK]
        odd = o[(2 * pair + 1) * BLOCK : (2 * pair + 2) * BLOCK]
        both = jnp.where(lane < HEAD_DIM, pltpu.roll(even, HEAD_DIM, 1), odd)
        out_ref[:, pair * LANES : (pair + 1) * LANES] = both.astype(jnp.bfloat16)


def attend(chosen, queries, bias, table):
    blocks, topk = chosen.shape
    rows = queries.shape[1]
    cols = rows // BLOCK * HEAD_DIM
    keys = topk * BLOCK
    return pl.pallas_call(
        functools.partial(attend_body, topk=topk),
        grid_spec=pltpu.PrefetchScalarGridSpec(
            num_scalar_prefetch=1,
            grid=(blocks,),
            in_specs=[
                pl.BlockSpec((1, rows, LANES), lambda i, s: (i, 0, 0)),
                pl.BlockSpec((1, 1, keys), lambda i, s: (i, 0, 0)),
                pl.BlockSpec(memory_space=pltpu.VMEM),
            ],
            out_specs=pl.BlockSpec((BLOCK, cols), lambda i, s: (i, 0)),
            scratch_shapes=[
                pltpu.VMEM((keys, LANES), jnp.bfloat16),
                pltpu.VMEM((rows, keys), jnp.float32),
                pltpu.VMEM((rows, keys), jnp.bfloat16),
            ],
        ),
        out_shape=jax.ShapeDtypeStruct((blocks * BLOCK, cols), jnp.bfloat16),
        compiler_params=pltpu.CompilerParams(
            dimension_semantics=("arbitrary",), vmem_limit_bytes=40 * 1024 * 1024
        ),
        name="attend",
    )(chosen, queries, bias, table)


def combine_body(x_ref, w_ref, out_ref):
    total = None
    for g in range(x_ref.shape[0]):
        part = jnp.dot(x_ref[g], w_ref[g], preferred_element_type=jnp.float32)
        part = part.astype(jnp.bfloat16).astype(jnp.float32)
        total = part if total is None else total + part
    out_ref[...] = total.astype(jnp.bfloat16)


def combine(parts, weights):
    peers, rows, depth = parts.shape
    cols = weights.shape[2]
    tile = 512
    return pl.pallas_call(
        combine_body,
        grid=(cols // tile,),
        in_specs=[
            pl.BlockSpec((peers, rows, depth), lambda j: (0, 0, 0)),
            pl.BlockSpec((peers, depth, tile), lambda j: (0, 0, j)),
        ],
        out_specs=pl.BlockSpec((rows, tile), lambda j: (0, j)),
        out_shape=jax.ShapeDtypeStruct((rows, cols), jnp.bfloat16),
        name="combine",
    )(parts, weights)


def rope_tables(row_count):
    positions = (lax.axis_index("kv") * row_count + jnp.arange(row_count)).astype(jnp.float32)
    lane = jnp.arange(LANES)
    freqs = ROPE_BASE ** (-(lane % HALF).astype(jnp.float32) / HALF)
    angles = positions[:, None] * freqs
    sign = jnp.where(lane % HEAD_DIM < HALF, -1.0, 1.0)
    return jnp.cos(angles), jnp.sin(angles) * sign


def shards(tokens, w_query, w_key, w_value, w_out, selection):
    row_count = tokens.shape[0]
    peers = lax.axis_size("tp")
    cosine, sine = rope_tables(row_count)
    codes, queries = project(tokens, w_query, w_key, w_value, cosine, sine)
    table = lax.all_gather(codes, "kv", axis=0, tiled=True)
    w_all = lax.all_gather(w_out, "tp", axis=0, tiled=False)
    chosen = selection[0]
    bias = jnp.where(jnp.repeat(chosen >= 0, BLOCK, axis=1), 0.0, -jnp.inf)
    attended = attend(chosen, queries, bias[:, None, :], table)
    tiles = attended.reshape(peers, row_count // peers, attended.shape[1])
    arrived = lax.all_to_all(tiles, "tp", split_axis=0, concat_axis=0, tiled=True)
    return combine(arrived, w_all)


def solution(mesh):
    placed = (
        P(("grp", "kv"), None),
        P(None, "tp"),
        P(None, "tp"),
        P(None, "tp"),
        P("tp", None),
        P("tp", ("grp", "kv"), None),
    )
    return jax.shard_map(
        shards, mesh=mesh, in_specs=placed, out_specs=P(("grp", "kv", "tp"), None), check_vma=False
    )
```

time: 270 us -> 181 us (0.67)
  waiting for transfers between devices: 161 us -> 0.75 us
  blocking collectives: 29.6 us -> 136 us
  matrix products: 28.6 us -> 0 us
  local copies, waits for them, and re-layouts: 31 us -> 4.14 us
  Pallas kernels: 0 us -> 23.7 us
  other arithmetic: 5.32 us -> 2.55 us
    all_gather x1, waiting for transfers between devices: 161 us -> 0.01 us  [shards(): w_all = lax.all_gather(w_out, 'tp', axis=0, tiled=False)]
    all_gather x0 -> x1, blocking collectives: none -> 124 us  [shards(): table = lax.all_gather(codes, 'kv', axis=0, tiled=True)]
    pallas_call x0 -> x3, Pallas kernels: none -> 23.7 us  [the longest x1 13.4 us: attend(): pl.pallas_call(functools.partial(attend_body, topk=topk), grid_spec=pltpu...]
    dot_general x5 -> x0, matrix products: 18 us -> none  [the longest x1 10.7 us: shards(): jnp.einsum('qhbk,qkd->qbhd', weights, picked_values, preferred_element_ty...]
    all_to_all x1, blocking collectives: 29.6 us -> 12.1 us  [shards(): lax.all_to_all(tiles, 'tp', split_axis=0, concat_axis=0, tiled=True)]
    all_gather x1 -> x0, local copies, waits for them, and re-layouts: 11.9 us -> none  [shards(): lax.all_gather(key_value, 'kv', axis=0, tiled=True)]
    sub x1 -> x0, matrix products: 10.6 us -> none  [shards(): expo = jnp.exp(scores - top_score)]
    slice x1 -> x0, local copies, waits for them, and re-layouts: 7.28 us -> none  [shards(): picked[..., :HEAD_DIM].reshape(blocks_here, TOPK * BLOCK, HEAD_DIM)]
  transfers between devices with their start and end apart: 1 -> 1, of which waited for: 1 -> 0; matrix products, arithmetic and copies ran while one was open for 2% -> 4% of each run, Pallas kernels for 0% -> 11%
where the time goes in v1:
time: 181 us
  blocking collectives  136 us (75%)
  Pallas kernels  23.7 us (13%)
  between operations  13.5 us (7%)
  local copies, waits for them, and re-layouts  4.14 us (2%)
  other arithmetic  2.55 us (1%)
    all_gather x1, blocking collectives, shards(): table = lax.all_gather(codes, 'kv', axis=0, tiled=True)  124 us
    pallas_call x1, Pallas kernels, attend(): pl.pallas_call(functools.partial(attend_body, topk=topk), grid_spec=pltpu...  13.4 us
    all_to_all x1, blocking collectives, shards(): lax.all_to_all(tiles, 'tp', split_axis=0, concat_axis=0, tiled=True)  12.1 us
    pallas_call x1, Pallas kernels, project(): pl.pallas_call(project_body, grid=(rows // tile,), in_specs=[pl.BlockSpec...  5.83 us
    pallas_call x1, Pallas kernels, combine(): pl.pallas_call(combine_body, grid=(cols // tile,), in_specs=[pl.BlockSpec...  4.52 us
    unnamed x6, local copies, waits for them, and re-layouts  3.92 us
  transfers between devices with their start and end apart: 1, of which 0 were waited for; matrix products, arithmetic and copies ran while one was open for 4% of the time, Pallas kernels for 11%

profile of v1, /device:TPU:33, one launch (start us, length us, event | category | flops | bytes accessed | tf_op | source)
XLA Modules:
  0.0 181.0 jit_solution(14509544290178172969)
XLA Ops:
  6.5 0.0 all-gather.4.cloned.1.call-start
  6.6 0.7 all-gather.4.cloned.1.call-update
  7.3 2.0 %copy.7.wk_ref = bf16[2048,64]{1,0:T(8,128)(2,1)} copy(bf16[2048,64]{0,1:T(8,128)(2,1)} %param.8) | data formatting | bytes 524288 | tf_op args[2]
  9.3 2.0 %copy.8.wv_ref = bf16[2048,64]{1,0:T(8,128)(2,1)} copy(bf16[2048,64]{0,1:T(8,128)(2,1)} %param.9) | data formatting | bytes 524288 | tf_op args[3]
  11.2 0.7 compare_select_fusion
  11.9 0.1 broadcast_in_dim.27
  12.0 0.1 select_n.46.bias_ref
  12.2 1.8 %fusion = (f32[512,128]{1,0:T(8,128)}, f32[512,128]{1,0:T(8,128)}) fusion(f32[128]{0:T(128)S(1)} %get-tuple-element.11, f32[128]{0:T(128)S(1)} %get-tuple-element.12, f32[512]{0:T(512)S(1)} %add_convert_fusion), kind=kLoop, calls=%fused_computation.2 | loop fusion | flops 131072 | bytes 527360 | tf_op jit(solution)/shard_map/mul | solution.py:199
  14.0 5.8 %project.1 = (s16[512,128]{1,0:T(8,128)(2,1)}, bf16[8,256,128]{2,1,0:T(8,128)(2,1)}) custom-call(bf16[512,2048]{1,0:T(8,128)(2,1)} %tok_ref.1, bf16[2048,256]{1,0:T(8,128)(2,1)} %wq_ref.1, bf16[2048,64]{1,0:T(8,128)(2,1)} %copy.7.wk_ref, bf16[2048,64]{1,0:T(8,128)(2,1)} %copy.8.wv_ref, f32[512,128]{1,0:T(8,128)} %get-tuple-element.10.cos_ref, ...), custom_call_target="tpu_custom_call" | custom-call | tf_op jit(solution)/shard_map/project/pallas_call | solution.py:80
  19.9 0.0 copy-start
  19.9 0.0 copy-start.1
  19.9 124.3 %all-gather.5.table_ref = s16[32768,128]{1,0:T(8,128)(2,1)S(1)} all-gather(s16[512,128]{1,0:T(8,128)(2,1)} %get-tuple-element.8), channel_id=1, replica_groups=mesh['grp'=2,'kv'=64,'tp'=4] {'kv'}, dimensions={0}, use_global_device_ids=true | all-gather | bytes 8519680 | tf_op jit(solution)/shard_map/all_gather | solution.py:207
  144.2 0.0 copy-done
  144.2 0.0 copy-done.1
  144.2 13.4 %attend.1 = bf16[512,256]{1,0:T(8,128)(2,1)S(1)} custom-call(s32[8,32]{1,0:T(8,128)S(1)} %bitcast.5, bf16[8,256,128]{2,1,0:T(8,128)(2,1)S(1)} %copy-done, f32[8,1,2048]{2,1,0:T(1,128)S(1)} %select_n.46.bias_ref, s16[32768,128]{1,0:T(8,128)(2,1)S(1)} %all-gather.5.table_ref), custom_call_target="tpu_custom_call" | custom-call | tf_op jit(solution)/shard_map/attend/pallas_call | solution.py:142
  157.6 12.1 %all_to_all.5.x_ref = bf16[4,128,256]{2,1,0:T(8,128)(2,1)} all-to-all(bf16[4,128,256]{2,1,0:T(8,128)(2,1)S(1)} %bitcast.4), channel_id=1, replica_groups=mesh['grp'=2,'kv'=64,'tp'=4] {'tp'}, dimensions={0} | all-to-all | bytes 524288 | tf_op jit(solution)/shard_map/all_to_all | solution.py:213
  169.7 0.0 all-gather.4.cloned.1.call-done
  169.7 4.5 %combine.1 = bf16[128,2048]{1,0:T(8,128)(2,1)} custom-call(bf16[4,128,256]{2,1,0:T(8,128)(2,1)} %all_to_all.5.x_ref, bf16[4,256,2048]{2,1,0:T(8,128)(2,1)} %bitcast.6), custom_call_target="tpu_custom_call" | custom-call | tf_op jit(solution)/shard_map/combine/pallas_call | solution.py:180
  (2 shorter events, 0.0 us)
Async XLA Ops:
  6.5 163.1 %all-gather.4.cloned.1.call-start = ((), (), s32[]{:S(2)}) async-start(), calls=%async_computation.1 | async-start | bytes 5242880 | tf_op jit(solution)/shard_map/all_gather | solution.py:208
  19.9 124.4 %copy-start = (bf16[8,256,128]{2,1,0:T(8,128)(2,1)S(1)}, bf16[8,256,128]{2,1,0:T(8,128)(2,1)}, u32[]{:S(2)}) copy-start(bf16[8,256,128]{2,1,0:T(8,128)(2,1)} %get-tuple-element.7.q_ref) | copy-start | bytes 1572868
  19.9 124.4 %copy-start.1 = (s32[1,8,32]{2,1,0:T(8,128)S(1)}, s32[1,8,32]{2,1,0:T(8,128)}, u32[]{:S(2)}) copy-start(s32[1,8,32]{2,1,0:T(8,128)} %param.11) | copy-start | bytes 3076
Sparse Core Ops, SparseCore 0:
  9.5 89.7 all-gather.3

commit v2 on v0

v2 whole, which is shorter than its diff:
```python
import jax
import jax.numpy as jnp
from jax import lax
from jax.experimental import pallas as pl
from jax.experimental.pallas import tpu as pltpu
from jax.sharding import PartitionSpec as P


HEAD_DIM = 64
BLOCK = 64
ROPE_BASE = 500000.0
LANES = 2 * HEAD_DIM
HALF = HEAD_DIM // 2


def encode(x):
    mag = jnp.abs(x)
    live = mag >= 2.0**-126
    safe = jnp.where(live, mag, 1.0)
    exponent = jnp.clip(jnp.floor(jnp.log2(safe)), -126.0, 126.0)
    half_exp = jnp.floor(exponent * 0.5)
    mantissa = safe * jnp.exp2(-half_exp) * jnp.exp2(half_exp - exponent)
    place = jnp.floor(mantissa * 128.0 - 127.5)
    carry = place >= 128.0
    place = jnp.where(carry, 0.0, place)
    exponent = jnp.where(carry, exponent + 1.0, exponent)
    code = (exponent + 1.0) * 256.0 + jnp.where(x < 0, 127.0 - place, 128.0 + place)
    return jnp.where(live, code, 128.0 - 126.0 * 256.0).astype(jnp.int32).astype(jnp.int16)


def decode(code):
    level = code.astype(jnp.int32).astype(jnp.float32) * (1.0 / 256.0)
    whole = jnp.floor(level)
    part = level - whole
    part = part - jnp.where(part < 0.5, 255.0 / 256.0, 0.0)
    return (part * jnp.exp2(whole)).astype(jnp.bfloat16)


def swap_halves(x, lane):
    return jnp.where(
        lane % HEAD_DIM < HALF,
        pltpu.roll(x, LANES - HALF, 1),
        pltpu.roll(x, HALF, 1),
    )


def turns(cos_ref, sin_ref, b):
    starts = cos_ref.shape[0] - BLOCK
    cos_at = cos_ref[b : b + 1, :]
    sin_at = sin_ref[b : b + 1, :]
    cos_in = cos_ref[starts:, :]
    sin_in = sin_ref[starts:, :]
    lane = lax.broadcasted_iota(jnp.int32, (BLOCK, LANES), 1)
    sign = jnp.where(lane % HEAD_DIM < HALF, -1.0, 1.0)
    return cos_at * cos_in - sin_at * sin_in, (sin_at * cos_in + cos_at * sin_in) * sign, lane


TILE = 4 * BLOCK
PART = 2 * BLOCK


def codes_body(
    tok_hbm, wk_hbm, wv_hbm, cos_hbm, sin_hbm, wo_hbm, code_hbm, sent_hbm,
    tok_ref, wkv_ref, cos_ref, sin_ref, code_ref, wo_ref, sems
):
    firsts = range(0, tok_ref.shape[0], PART)
    peers = sent_hbm.shape[0]
    at = iter(range(5 + 2 * len(firsts) + peers))
    small = [
        pltpu.make_async_copy(wk_hbm, wkv_ref.at[:HEAD_DIM], sems.at[next(at)]),
        pltpu.make_async_copy(wv_hbm, wkv_ref.at[HEAD_DIM:], sems.at[next(at)]),
        pltpu.make_async_copy(cos_hbm, cos_ref, sems.at[next(at)]),
        pltpu.make_async_copy(sin_hbm, sin_ref, sems.at[next(at)]),
    ]
    spans = [pl.ds(first, PART) for first in firsts]
    reads = [
        pltpu.make_async_copy(tok_hbm.at[span], tok_ref.at[span], sems.at[next(at)]) for span in spans
    ]
    writes = [
        pltpu.make_async_copy(code_ref.at[span], code_hbm.at[span], sems.at[next(at)]) for span in spans
    ]
    copies = [
        pltpu.make_async_copy(wo_ref, sent_hbm.at[peer], sems.at[next(at)]) for peer in range(peers)
    ]
    stage = pltpu.make_async_copy(wo_hbm, wo_ref, sems.at[next(at)])
    for move in small + reads[:1] + [stage] + reads[1:]:
        move.start()
    for move in small:
        move.wait()
    for first, read, write in zip(firsts, reads, writes):
        read.wait()
        if first == PART:
            stage.wait()
            for move in copies:
                move.start()
        kv_all = lax.dot_general(
            tok_ref[first : first + PART, :],
            wkv_ref[...],
            (((1,), (1,)), ((), ())),
            preferred_element_type=jnp.float32,
        )
        for at in range(0, PART, BLOCK):
            cosine, sine, lane = turns(cos_ref, sin_ref, (first + at) // BLOCK)
            kv = kv_all[at : at + BLOCK]
            kv = jnp.where(lane < HEAD_DIM, kv * cosine + swap_halves(kv, lane) * sine, kv)
            code_ref[first + at : first + at + BLOCK, :] = encode(
                kv.astype(jnp.bfloat16).astype(jnp.float32)
            )
        write.start()
    for move in writes + copies:
        move.wait()


def project_codes(tokens, w_key, w_value, cosine, sine, w_out, peers):
    rows, width = tokens.shape
    far = pl.BlockSpec(memory_space=pltpu.HBM)
    return pl.pallas_call(
        codes_body,
        in_specs=[far] * 6,
        out_specs=[far] * 2,
        out_shape=[
            jax.ShapeDtypeStruct((rows, LANES), jnp.int16),
            jax.ShapeDtypeStruct((peers, *w_out.shape), jnp.bfloat16),
        ],
        scratch_shapes=[
            pltpu.VMEM((rows, width), jnp.bfloat16),
            pltpu.VMEM((LANES, width), jnp.bfloat16),
            pltpu.VMEM(cosine.shape, jnp.float32),
            pltpu.VMEM(sine.shape, jnp.float32),
            pltpu.VMEM((rows, LANES), jnp.int16),
            pltpu.VMEM(w_out.shape, jnp.bfloat16),
            pltpu.SemaphoreType.DMA((5 + 2 * (rows // PART) + peers,)),
        ],
        compiler_params=pltpu.CompilerParams(vmem_limit_bytes=63 * 1024 * 1024),
        name="project_codes",
    )(tokens, w_key.T, w_value.T, cosine, sine, w_out)


def queries_body(tok_ref, wq_ref, cos_ref, sin_ref, q_ref):
    for first in range(0, tok_ref.shape[0], TILE):
        q_all = jnp.dot(
            tok_ref[first : first + TILE, :], wq_ref[...], preferred_element_type=jnp.float32
        )
        for at in range(0, TILE, BLOCK):
            b = (first + at) // BLOCK
            cosine, sine, lane = turns(cos_ref, sin_ref, b)
            for pair in range(q_all.shape[1] // LANES):
                q = q_all[at : at + BLOCK, pair * LANES : (pair + 1) * LANES]
                q = q * cosine + swap_halves(q, lane) * sine
                q = q.astype(jnp.bfloat16).astype(jnp.float32) * HEAD_DIM**-0.5
                even = 2 * pair * BLOCK
                odd = even + BLOCK
                q_ref[b, even:odd, :] = jnp.where(lane < HEAD_DIM, q, 0.0).astype(jnp.bfloat16)
                q_ref[b, odd : odd + BLOCK, :] = jnp.where(
                    lane < HEAD_DIM, pltpu.roll(q, HEAD_DIM, 1), 0.0
                ).astype(jnp.bfloat16)


def project_queries(tokens, w_query, cosine, sine):
    rows = tokens.shape[0]
    heads = w_query.shape[1] // HEAD_DIM
    whole = pl.BlockSpec(memory_space=pltpu.VMEM)
    return pl.pallas_call(
        queries_body,
        in_specs=[whole] * 4,
        out_specs=whole,
        out_shape=jax.ShapeDtypeStruct((rows // BLOCK, heads * BLOCK, LANES), jnp.bfloat16),
        compiler_params=pltpu.CompilerParams(vmem_limit_bytes=32 * 1024 * 1024),
        name="project_queries",
    )(tokens, w_query, cosine, sine)


SLOTS = 4


def attend_body(sel_ref, q_ref, table_ref, out_ref, *scratch):
    kv_refs, s_refs, p_refs = scratch[:SLOTS], scratch[SLOTS : 2 * SLOTS], scratch[2 * SLOTS :]
    blocks, topk = sel_ref.shape
    rows = q_ref.shape[1]
    keys = topk * BLOCK
    chunk = 16
    row = lax.broadcasted_iota(jnp.int32, (chunk, LANES), 0)
    col = lax.broadcasted_iota(jnp.int32, (chunk, LANES), 1)
    key_at = lax.broadcasted_iota(jnp.int32, (1, keys), 1)
    half_lane = lax.broadcasted_iota(jnp.int32, (BLOCK, LANES), 1) < HEAD_DIM

    def load(k, b):
        used = jnp.int32(0)
        for t in range(topk):
            block = sel_ref[b, t]
            used += (block >= 0).astype(jnp.int32)
            at = pl.multiple_of(jnp.maximum(block, 0) * BLOCK, BLOCK)
            kv_refs[k][t * BLOCK : (t + 1) * BLOCK, :] = decode(table_ref[pl.ds(at, BLOCK), :])
        return jnp.where(key_at < used * BLOCK, 0.0, -jnp.inf)

    def score(k, b):
        s_refs[k][...] = lax.dot_general(
            q_ref[b], kv_refs[k][...], (((1,), (1,)), ((), ())), preferred_element_type=jnp.float32
        )

    def soften(k, bias):
        sums = []
        for r in range(0, rows, chunk):
            s = s_refs[k][r : r + chunk, :] + bias
            first = jnp.where((col < BLOCK) & (col > row + r % BLOCK), -jnp.inf, s[:, :LANES])
            s = jnp.concatenate([first, s[:, LANES:]], axis=1)
            e = jnp.exp(s - jnp.max(s, axis=1, keepdims=True))
            sums.append(jnp.sum(e, axis=1, keepdims=True))
            p_refs[k][r : r + chunk, :] = e.astype(jnp.bfloat16)
        return jnp.concatenate(sums, axis=0)

    def finish(k, b, sums):
        o = jnp.dot(p_refs[k][...], kv_refs[k][...], preferred_element_type=jnp.float32) / sums
        at = pl.multiple_of(b * BLOCK, BLOCK)
        for pair in range(rows // BLOCK // 2):
            even = o[2 * pair * BLOCK : (2 * pair + 1) * BLOCK]
            odd = o[(2 * pair + 1) * BLOCK : (2 * pair + 2) * BLOCK]
            both = jnp.where(half_lane, pltpu.roll(even, HEAD_DIM, 1), odd)
            out_ref[pl.ds(at, BLOCK), pair * LANES : (pair + 1) * LANES] = both.astype(jnp.bfloat16)

    def step(i, _):
        first = i * SLOTS
        biases = [load(0, first)]
        score(0, first)
        for k in range(SLOTS):
            if k + 1 < SLOTS:
                biases.append(load(k + 1, first + k + 1))
            sums = soften(k, biases[k])
            if k + 1 < SLOTS:
                score(k + 1, first + k + 1)
            finish(k, first + k, sums)
        return 0

    lax.fori_loop(0, blocks // SLOTS, step, 0)


def attend(chosen, queries, table):
    blocks, topk = chosen.shape
    rows = queries.shape[1]
    cols = rows // BLOCK * HEAD_DIM
    keys = topk * BLOCK
    whole = pl.BlockSpec(memory_space=pltpu.VMEM)
    return pl.pallas_call(
        attend_body,
        in_specs=[pl.BlockSpec(memory_space=pltpu.SMEM), whole, whole],
        out_specs=whole,
        out_shape=jax.ShapeDtypeStruct((blocks * BLOCK, cols), jnp.bfloat16),
        scratch_shapes=[pltpu.VMEM((keys, LANES), jnp.bfloat16) for _ in range(SLOTS)]
        + [pltpu.VMEM((rows, keys), jnp.float32) for _ in range(SLOTS)]
        + [pltpu.VMEM((rows, keys), jnp.bfloat16) for _ in range(SLOTS)],
        compiler_params=pltpu.CompilerParams(vmem_limit_bytes=40 * 1024 * 1024),
        name="attend",
    )(chosen, queries, table)


COLS = 512


def keep_body(peer_ref, x_ref, w_ref, out_ref):
    rows = out_ref.shape[0]
    x = x_ref[pl.ds(pl.multiple_of(peer_ref[0] * rows, rows), rows), :]
    for j in range(0, out_ref.shape[1], COLS):
        part = jnp.dot(x, w_ref[:, j : j + COLS], preferred_element_type=jnp.float32)
        out_ref[:, j : j + COLS] = part.astype(jnp.bfloat16)


def keep(peer, attended, w_out, rows):
    whole = pl.BlockSpec(memory_space=pltpu.VMEM)
    return pl.pallas_call(
        keep_body,
        in_specs=[pl.BlockSpec(memory_space=pltpu.SMEM), whole, whole],
        out_specs=whole,
        out_shape=jax.ShapeDtypeStruct((rows, w_out.shape[1]), jnp.bfloat16),
        compiler_params=pltpu.CompilerParams(vmem_limit_bytes=16 * 1024 * 1024),
        name="keep",
    )(peer, attended, w_out)


def combine_body(peer_ref, own_ref, x_ref, w_ref, out_ref):
    peers = x_ref.shape[0]
    others = [lax.rem(peer_ref[0] + away, peers) for away in range(1, peers)]
    parts = [x_ref[g] for g in others]
    for j in range(0, out_ref.shape[1], COLS):
        total = own_ref[:, j : j + COLS].astype(jnp.float32)
        for g, x in zip(others, parts):
            part = jnp.dot(x, w_ref[g, :, j : j + COLS], preferred_element_type=jnp.float32)
            total = total + part.astype(jnp.bfloat16).astype(jnp.float32)
        out_ref[:, j : j + COLS] = total.astype(jnp.bfloat16)


def combine(peer, own, parts, weights):
    whole = pl.BlockSpec(memory_space=pltpu.VMEM)
    return pl.pallas_call(
        combine_body,
        in_specs=[pl.BlockSpec(memory_space=pltpu.SMEM)] + [whole] * 3,
        out_specs=whole,
        out_shape=jax.ShapeDtypeStruct(own.shape, jnp.bfloat16),
        compiler_params=pltpu.CompilerParams(vmem_limit_bytes=16 * 1024 * 1024),
        name="combine",
    )(peer, own, parts, weights)


def rope_tables(row_count):
    blocks = row_count // BLOCK
    row = jnp.arange(blocks + BLOCK)
    start = lax.axis_index("kv") * row_count + row * BLOCK
    positions = jnp.where(row < blocks, start, row - blocks).astype(jnp.float32)
    lane = jnp.arange(LANES)
    freqs = ROPE_BASE ** (-(lane % HALF).astype(jnp.float32) / HALF)
    angles = positions[:, None] * freqs
    return jnp.cos(angles), jnp.sin(angles)


def exchange(tiles):
    return lax.all_to_all(tiles, "tp", split_axis=0, concat_axis=0, tiled=True)


def shards(tokens, w_query, w_key, w_value, w_out, selection):
    row_count = tokens.shape[0]
    peers = lax.axis_size("tp")
    peer = lax.axis_index("tp").reshape(1)
    cosine, sine = rope_tables(row_count)
    codes, w_sent = project_codes(tokens, w_key, w_value, cosine, sine, w_out, peers)
    weights = exchange(w_sent)
    queries = project_queries(tokens, w_query, cosine, sine)
    table = lax.all_gather(codes, "kv", axis=0, tiled=True)
    attended = attend(selection[0], queries, table)
    attended, weights = lax.optimization_barrier((attended, weights))
    arrived = exchange(attended.reshape(peers, row_count // peers, attended.shape[1]))
    own = keep(peer, attended, w_out, row_count // peers)
    return combine(peer, own, arrived, weights)


def solution(mesh):
    placed = (
        P(("grp", "kv"), None),
        P(None, "tp"),
        P(None, "tp"),
        P(None, "tp"),
        P("tp", None),
        P("tp", ("grp", "kv"), None),
    )
    return jax.shard_map(
        shards, mesh=mesh, in_specs=placed, out_specs=P(("grp", "kv", "tp"), None), check_vma=False
    )
```

time: 270 us -> 162 us (0.60)
  waiting for transfers between devices: 161 us -> 4.76 us
  blocking collectives: 29.6 us -> 124 us
  local copies, waits for them, and re-layouts: 31 us -> 0.04 us
  matrix products: 28.6 us -> 0 us
  Pallas kernels: 0 us -> 21 us
  between operations: 13.6 us -> 0.11 us
  starting transfers between devices: 0.01 us -> 10.8 us
  other arithmetic: 5.32 us -> 0.86 us
    all_gather x1 -> x0, waiting for transfers between devices: 161 us -> none  [shards(): lax.all_gather(key_value, 'kv', axis=0, tiled=True)]
    all_gather x0 -> x1, blocking collectives: none -> 124 us  [shards(): table = lax.all_gather(codes, 'kv', axis=0, tiled=True)]
    all_to_all x1 -> x0, blocking collectives: 29.6 us -> none  [sum_at_owner(): lax.all_to_all(tiles, axis, split_axis=0, concat_axis=0, tiled=True)]
    pallas_call x0 -> x5, Pallas kernels: none -> 21 us  [the longest x1 10.7 us: attend(): pl.pallas_call(attend_body, in_specs=[pl.BlockSpec(memory_space=pltpu.SME...]
    dot_general x5 -> x0, matrix products: 18 us -> none  [the longest x1 10.7 us: shards(): jnp.einsum('qhbk,qkd->qbhd', weights, picked_values, preferred_element_ty...]
    all_gather x1 -> x0, local copies, waits for them, and re-layouts: 11.9 us -> none  [shards(): lax.all_gather(key_value, 'kv', axis=0, tiled=True)]
    all_to_all x0 -> x2, starting transfers between devices: none -> 10.8 us  [exchange(): return lax.all_to_all(tiles, 'tp', split_axis=0, concat_axis=0, tiled=True)]
    sub x1 -> x0, matrix products: 10.6 us -> none  [shards(): expo = jnp.exp(scores - top_score)]
  transfers between devices with their start and end apart: 1 -> 2, of which waited for: 1 -> 1; matrix products, arithmetic and copies ran while one was open for 2% -> 0% of each run, Pallas kernels for 0% -> 8%
where the time goes in v2:
time: 162 us
  blocking collectives  124 us (77%)
  Pallas kernels  21 us (13%)
  starting transfers between devices  10.8 us (7%)
  waiting for transfers between devices  4.76 us (3%)
    all_gather x1, blocking collectives, shards(): table = lax.all_gather(codes, 'kv', axis=0, tiled=True)  124 us
    all_to_all x2, starting transfers between devices, exchange(): return lax.all_to_all(tiles, 'tp', split_axis=0, concat_axis=0, tiled=True)  10.8 us
    pallas_call x1, Pallas kernels, attend(): pl.pallas_call(attend_body, in_specs=[pl.BlockSpec(memory_space=pltpu.SME...  10.7 us
    all_to_all x2, waiting for transfers between devices, exchange(): return lax.all_to_all(tiles, 'tp', split_axis=0, concat_axis=0, tiled=True)  4.76 us
    pallas_call x1, Pallas kernels, project_codes(): pl.pallas_call(codes_body, in_specs=[far] * 6, out_specs=[far] * 2, out_s...  4.25 us
    pallas_call x1, Pallas kernels, combine(): pl.pallas_call(combine_body, in_specs=[pl.BlockSpec(memory_space=pltpu.SM...  3.65 us
  transfers between devices with their start and end apart: 2, of which 1 were waited for; matrix products, arithmetic and copies ran while one was open for 0% of the time, Pallas kernels for 8%

profile of v2, /device:TPU:33, one launch (start us, length us, event | category | flops | bytes accessed | tf_op | source)
XLA Modules:
  0.0 161.5 jit_solution(17414398008241595004)
XLA Ops:
  0.0 0.8 multiply_sine_fusion
  0.9 4.3 %project_codes.1 = (s16[512,128]{1,0:T(8,128)(2,1)}, bf16[4,256,2048]{2,1,0:T(8,128)(2,1)}) custom-call(bf16[512,2048]{1,0:T(8,128)(2,1)} %tok_hbm.1, bf16[64,2048]{1,0:T(8,128)(2,1)} %bitcast.6, bf16[64,2048]{1,0:T(8,128)(2,1)} %bitcast.7, f32[72,128]{1,0:T(8,128)} %get-tuple-element.14.cos_ref.cos_hbm, f32[72,128]{1,0:T(8,128)} %get-tuple-element.13.sin_ref.sin_hbm, ...), custom_call_target="tpu_custom_call" | custom-call | tf_op jit(solution)/shard_map/project_codes/pallas_call | solution.py:117
  5.1 0.0 copy-start
  5.1 0.0 copy-start.2
  5.2 0.0 copy-start.3
  5.2 0.0 copy-start.4
  5.2 0.0 copy-start.6
  5.2 5.4 %all-to-all-start = ((bf16[4,256,2048]{2,1,0:T(8,128)(2,1)}), bf16[4,256,2048]{2,1,0:T(8,128)(2,1)}, u32[]{:S(2)}, u32[]{:S(2)}) async-start(bf16[4,256,2048]{2,1,0:T(8,128)(2,1)} %get-tuple-element.10), calls=%async_computation | async-start | bytes 8388608 | tf_op jit(solution)/shard_map/all_to_all | solution.py:315
  10.6 0.0 copy-done
  10.6 0.0 copy-done.2
  10.6 0.0 copy-done.3
  10.6 0.0 copy-done.4
  10.6 1.1 project_queries.1.q_ref
  11.7 0.0 copy-done.6
  11.7 0.0 copy-start.5
  11.7 124.0 %all-gather.1.table_ref = s16[32768,128]{1,0:T(8,128)(2,1)S(1)} all-gather(s16[512,128]{1,0:T(8,128)(2,1)S(1)} %copy-done.6), channel_id=1, replica_groups=mesh['grp'=2,'kv'=64,'tp'=4] {'kv'}, dimensions={0}, use_global_device_ids=true | all-gather | bytes 8519680 | tf_op jit(solution)/shard_map/all_gather | solution.py:326
  135.7 0.0 copy-done.5
  135.7 10.7 %attend.1.x_ref = bf16[512,256]{1,0:T(8,128)(2,1)} custom-call(s32[8,32]{1,0:T(8,128)S(1)} %bitcast.5, bf16[8,256,128]{2,1,0:T(8,128)(2,1)S(1)} %project_queries.1.q_ref, s16[32768,128]{1,0:T(8,128)(2,1)S(1)} %all-gather.1.table_ref), custom_call_target="tpu_custom_call" | custom-call | tf_op jit(solution)/shard_map/attend/pallas_call | solution.py:243
  146.4 0.0 all-to-all-done.w_ref
  146.4 5.4 %all-to-all-start.1 = ((bf16[4,128,256]{2,1,0:T(8,128)(2,1)}), bf16[4,128,256]{2,1,0:T(8,128)(2,1)S(1)}, u32[]{:S(2)}, u32[]{:S(2)}) async-start(bf16[4,128,256]{2,1,0:T(8,128)(2,1)} %bitcast.4), calls=%async_computation.1 | async-start | bytes 524288 | tf_op jit(solution)/shard_map/all_to_all | solution.py:315
  151.8 0.0 copy-done.1
  151.8 1.3 keep.1.own_ref
  153.1 4.8 %all-to-all-done.1.x_ref = bf16[4,128,256]{2,1,0:T(8,128)(2,1)S(1)} async-done(((bf16[4,128,256]{2,1,0:T(8,128)(2,1)}), bf16[4,128,256]{2,1,0:T(8,128)(2,1)S(1)}, u32[]{:S(2)}, u32[]{:S(2)}) %all-to-all-start.1) | async-done | bytes 262176 | tf_op jit(solution)/shard_map/all_to_all | solution.py:315
  157.9 3.6 %combine.1 = bf16[128,2048]{1,0:T(8,128)(2,1)} custom-call(s32[1]{0:T(128)} %bitcast.peer_ref, bf16[128,2048]{1,0:T(8,128)(2,1)S(1)} %keep.1.own_ref, bf16[4,128,256]{2,1,0:T(8,128)(2,1)S(1)} %all-to-all-done.1.x_ref, bf16[4,256,2048]{2,1,0:T(8,128)(2,1)} %all-to-all-done.w_ref), custom_call_target="tpu_custom_call" | custom-call | tf_op jit(solution)/shard_map/combine/pallas_call | solution.py:293
  (3 shorter events, 0.0 us)
Async XLA Ops:
  5.1 5.5 %copy-start = (bf16[512,2048]{1,0:T(8,128)(2,1)S(1)}, bf16[512,2048]{1,0:T(8,128)(2,1)}, u32[]{:S(2)}) copy-start(bf16[512,2048]{1,0:T(8,128)(2,1)} %tok_hbm.1) | copy-start | bytes 6291460
  5.1 5.4 %copy-start.2 = (bf16[2048,256]{1,0:T(8,128)(2,1)S(1)}, bf16[2048,256]{1,0:T(8,128)(2,1)}, u32[]{:S(2)}) copy-start(bf16[2048,256]{1,0:T(8,128)(2,1)} %wq_ref.1) | copy-start | bytes 3145732
  5.2 5.4 %copy-start.3 = (f32[72,128]{1,0:T(8,128)S(1)}, f32[72,128]{1,0:T(8,128)}, u32[]{:S(2)}) copy-start(f32[72,128]{1,0:T(8,128)} %get-tuple-element.13.sin_ref.sin_hbm) | copy-start | bytes 110596
  5.2 5.4 %copy-start.4 = (f32[72,128]{1,0:T(8,128)S(1)}, f32[72,128]{1,0:T(8,128)}, u32[]{:S(2)}) copy-start(f32[72,128]{1,0:T(8,128)} %get-tuple-element.14.cos_ref.cos_hbm) | copy-start | bytes 110596
  5.2 6.5 %copy-start.6 = (s16[512,128]{1,0:T(8,128)(2,1)S(1)}, s16[512,128]{1,0:T(8,128)(2,1)}, u32[]{:S(2)}) copy-start(s16[512,128]{1,0:T(8,128)(2,1)} %get-tuple-element.9) | copy-start | bytes 393220
  5.2 141.2 %all-to-all-start = ((bf16[4,256,2048]{2,1,0:T(8,128)(2,1)}), bf16[4,256,2048]{2,1,0:T(8,128)(2,1)}, u32[]{:S(2)}, u32[]{:S(2)}) async-start(bf16[4,256,2048]{2,1,0:T(8,128)(2,1)} %get-tuple-element.10), calls=%async_computation | async-start | bytes 8388608 | tf_op jit(solution)/shard_map/all_to_all | solution.py:315
  11.7 124.0 %copy-start.5 = (s32[1,8,32]{2,1,0:T(8,128)S(1)}, s32[1,8,32]{2,1,0:T(8,128)}, u32[]{:S(2)}) copy-start(s32[1,8,32]{2,1,0:T(8,128)} %param.11) | copy-start | bytes 3076
  135.7 16.1 %copy-start.1 = (bf16[256,2048]{1,0:T(8,128)(2,1)S(1)}, bf16[256,2048]{1,0:T(8,128)(2,1)}, u32[]{:S(2)}) copy-start(bf16[256,2048]{1,0:T(8,128)(2,1)} %w_ref.1) | copy-start | bytes 3145732
  146.4 11.4 %all-to-all-start.1 = ((bf16[4,128,256]{2,1,0:T(8,128)(2,1)}), bf16[4,128,256]{2,1,0:T(8,128)(2,1)S(1)}, u32[]{:S(2)}, u32[]{:S(2)}) async-start(bf16[4,128,256]{2,1,0:T(8,128)(2,1)} %bitcast.4), calls=%async_computation.1 | async-start | bytes 524288 | tf_op jit(solution)/shard_map/all_to_all | solution.py:315

commit v3 on v2

--- a/solution.py
+++ b/solution.py
@@ -276,25 +276,45 @@
     )(peer, attended, w_out)
 
 
-def combine_body(peer_ref, own_ref, x_ref, w_ref, out_ref):
+def combine_body(peer_ref, own_ref, x_ref, all_hbm, out_ref, w_ref, sum_ref, sems):
     peers = x_ref.shape[0]
     others = [lax.rem(peer_ref[0] + away, peers) for away in range(1, peers)]
-    parts = [x_ref[g] for g in others]
-    for j in range(0, out_ref.shape[1], COLS):
-        total = own_ref[:, j : j + COLS].astype(jnp.float32)
-        for g, x in zip(others, parts):
-            part = jnp.dot(x, w_ref[g, :, j : j + COLS], preferred_element_type=jnp.float32)
-            total = total + part.astype(jnp.bfloat16).astype(jnp.float32)
-        out_ref[:, j : j + COLS] = total.astype(jnp.bfloat16)
+    moves = [
+        pltpu.make_async_copy(all_hbm.at[g], w_ref.at[n], sems.at[n]) for n, g in enumerate(others)
+    ]
+    for move in moves:
+        move.start()
+    for n, (g, move) in enumerate(zip(others, moves)):
+        x = x_ref[g]
+        move.wait()
+        for j in range(0, out_ref.shape[1], COLS):
+            part = jnp.dot(x, w_ref[n, :, j : j + COLS], preferred_element_type=jnp.float32)
+            before = own_ref[:, j : j + COLS].astype(jnp.float32) if n == 0 else sum_ref[:, j : j + COLS]
+            total = before + part.astype(jnp.bfloat16).astype(jnp.float32)
+            if n + 1 < len(others):
+                sum_ref[:, j : j + COLS] = total
+            else:
+                out_ref[:, j : j + COLS] = total.astype(jnp.bfloat16)
 
 
 def combine(peer, own, parts, weights):
     whole = pl.BlockSpec(memory_space=pltpu.VMEM)
+    others = weights.shape[0] - 1
     return pl.pallas_call(
         combine_body,
-        in_specs=[pl.BlockSpec(memory_space=pltpu.SMEM)] + [whole] * 3,
+        in_specs=[
+            pl.BlockSpec(memory_space=pltpu.SMEM),
+            whole,
+            whole,
+            pl.BlockSpec(memory_space=pltpu.HBM),
+        ],
         out_specs=whole,
         out_shape=jax.ShapeDtypeStruct(own.shape, jnp.bfloat16),
+        scratch_shapes=[
+            pltpu.VMEM((others, *weights.shape[1:]), jnp.bfloat16),
+            pltpu.VMEM(own.shape, jnp.float32),
+            pltpu.SemaphoreType.DMA((others,)),
+        ],
         compiler_params=pltpu.CompilerParams(vmem_limit_bytes=16 * 1024 * 1024),
         name="combine",
     )(peer, own, parts, weights)

time: 162 us -> 161 us (level)
  no operation moved by 1% of the time
where the time goes in v3:
time: 161 us
  blocking collectives  124 us (77%)
  Pallas kernels  20.3 us (13%)
  starting transfers between devices  10.8 us (7%)
  waiting for transfers between devices  4.76 us (3%)
    all_gather x1, blocking collectives, shards(): table = lax.all_gather(codes, 'kv', axis=0, tiled=True)  124 us
    all_to_all x2, starting transfers between devices, exchange(): return lax.all_to_all(tiles, 'tp', split_axis=0, concat_axis=0, tiled=True)  10.8 us
    pallas_call x1, Pallas kernels, attend(): pl.pallas_call(attend_body, in_specs=[pl.BlockSpec(memory_space=pltpu.SME...  10.7 us
    all_to_all x2, waiting for transfers between devices, exchange(): return lax.all_to_all(tiles, 'tp', split_axis=0, concat_axis=0, tiled=True)  4.76 us
    pallas_call x1, Pallas kernels, project_codes(): pl.pallas_call(codes_body, in_specs=[far] * 6, out_specs=[far] * 2, out_s...  4.25 us
  transfers between devices with their start and end apart: 2, of which 1 were waited for; matrix products, arithmetic and copies ran while one was open for 0% of the time, Pallas kernels for 8%

profile of v3, /device:TPU:33, one launch (start us, length us, event | category | flops | bytes accessed | tf_op | source)
XLA Modules:
  0.0 160.9 jit_solution(14047937204142707056)
XLA Ops:
  0.0 0.8 multiply_sine_fusion
  0.9 4.3 %project_codes.1 = (s16[512,128]{1,0:T(8,128)(2,1)}, bf16[4,256,2048]{2,1,0:T(8,128)(2,1)}) custom-call(bf16[512,2048]{1,0:T(8,128)(2,1)} %tok_hbm.1, bf16[64,2048]{1,0:T(8,128)(2,1)} %bitcast.6, bf16[64,2048]{1,0:T(8,128)(2,1)} %bitcast.7, f32[72,128]{1,0:T(8,128)} %get-tuple-element.14.cos_ref.cos_hbm, f32[72,128]{1,0:T(8,128)} %get-tuple-element.13.sin_ref.sin_hbm, ...), custom_call_target="tpu_custom_call" | custom-call | tf_op jit(solution)/shard_map/project_codes/pallas_call | solution.py:117
  5.1 0.0 copy-start
  5.1 0.0 copy-start.2
  5.2 0.0 copy-start.3
  5.2 0.0 copy-start.4
  5.2 0.0 copy-start.6
  5.2 5.4 %all-to-all-start = ((bf16[4,256,2048]{2,1,0:T(8,128)(2,1)}), bf16[4,256,2048]{2,1,0:T(8,128)(2,1)}, u32[]{:S(2)}, u32[]{:S(2)}) async-start(bf16[4,256,2048]{2,1,0:T(8,128)(2,1)} %get-tuple-element.10), calls=%async_computation | async-start | bytes 8388608 | tf_op jit(solution)/shard_map/all_to_all | solution.py:335
  10.6 0.0 copy-done
  10.6 0.0 copy-done.2
  10.6 0.0 copy-done.3
  10.6 0.0 copy-done.4
  10.6 1.1 project_queries.1.q_ref
  11.7 0.0 copy-done.6
  11.7 0.0 copy-start.5
  11.7 124.0 %all-gather.1.table_ref = s16[32768,128]{1,0:T(8,128)(2,1)S(1)} all-gather(s16[512,128]{1,0:T(8,128)(2,1)S(1)} %copy-done.6), channel_id=1, replica_groups=mesh['grp'=2,'kv'=64,'tp'=4] {'kv'}, dimensions={0}, use_global_device_ids=true | all-gather | bytes 8519680 | tf_op jit(solution)/shard_map/all_gather | solution.py:346
  135.7 0.0 copy-done.5
  135.7 10.7 %attend.1.x_ref = bf16[512,256]{1,0:T(8,128)(2,1)} custom-call(s32[8,32]{1,0:T(8,128)S(1)} %bitcast.5, bf16[8,256,128]{2,1,0:T(8,128)(2,1)S(1)} %project_queries.1.q_ref, s16[32768,128]{1,0:T(8,128)(2,1)S(1)} %all-gather.1.table_ref), custom_call_target="tpu_custom_call" | custom-call | tf_op jit(solution)/shard_map/attend/pallas_call | solution.py:243
  146.4 0.0 all-to-all-done.all_hbm
  146.4 5.4 %all-to-all-start.1 = ((bf16[4,128,256]{2,1,0:T(8,128)(2,1)}), bf16[4,128,256]{2,1,0:T(8,128)(2,1)S(1)}, u32[]{:S(2)}, u32[]{:S(2)}) async-start(bf16[4,128,256]{2,1,0:T(8,128)(2,1)} %bitcast.4), calls=%async_computation.1 | async-start | bytes 524288 | tf_op jit(solution)/shard_map/all_to_all | solution.py:335
  151.8 0.0 copy-done.1
  151.8 1.3 keep.1.own_ref
  153.1 4.8 %all-to-all-done.1.x_ref = bf16[4,128,256]{2,1,0:T(8,128)(2,1)S(1)} async-done(((bf16[4,128,256]{2,1,0:T(8,128)(2,1)}), bf16[4,128,256]{2,1,0:T(8,128)(2,1)S(1)}, u32[]{:S(2)}, u32[]{:S(2)}) %all-to-all-start.1) | async-done | bytes 262176 | tf_op jit(solution)/shard_map/all_to_all | solution.py:335
  157.9 3.0 %combine.1 = bf16[128,2048]{1,0:T(8,128)(2,1)} custom-call(s32[1]{0:T(128)} %bitcast.peer_ref, bf16[128,2048]{1,0:T(8,128)(2,1)S(1)} %keep.1.own_ref, bf16[4,128,256]{2,1,0:T(8,128)(2,1)S(1)} %all-to-all-done.1.x_ref, bf16[4,256,2048]{2,1,0:T(8,128)(2,1)} %all-to-all-done.all_hbm), custom_call_target="tpu_custom_call" | custom-call | tf_op jit(solution)/shard_map/combine/pallas_call | solution.py:303
  (3 shorter events, 0.0 us)
Async XLA Ops:
  5.1 5.5 %copy-start = (bf16[512,2048]{1,0:T(8,128)(2,1)S(1)}, bf16[512,2048]{1,0:T(8,128)(2,1)}, u32[]{:S(2)}) copy-start(bf16[512,2048]{1,0:T(8,128)(2,1)} %tok_hbm.1) | copy-start | bytes 6291460
  5.1 5.4 %copy-start.2 = (bf16[2048,256]{1,0:T(8,128)(2,1)S(1)}, bf16[2048,256]{1,0:T(8,128)(2,1)}, u32[]{:S(2)}) copy-start(bf16[2048,256]{1,0:T(8,128)(2,1)} %wq_ref.1) | copy-start | bytes 3145732
  5.2 5.4 %copy-start.3 = (f32[72,128]{1,0:T(8,128)S(1)}, f32[72,128]{1,0:T(8,128)}, u32[]{:S(2)}) copy-start(f32[72,128]{1,0:T(8,128)} %get-tuple-element.13.sin_ref.sin_hbm) | copy-start | bytes 110596
  5.2 5.4 %copy-start.4 = (f32[72,128]{1,0:T(8,128)S(1)}, f32[72,128]{1,0:T(8,128)}, u32[]{:S(2)}) copy-start(f32[72,128]{1,0:T(8,128)} %get-tuple-element.14.cos_ref.cos_hbm) | copy-start | bytes 110596
  5.2 6.5 %copy-start.6 = (s16[512,128]{1,0:T(8,128)(2,1)S(1)}, s16[512,128]{1,0:T(8,128)(2,1)}, u32[]{:S(2)}) copy-start(s16[512,128]{1,0:T(8,128)(2,1)} %get-tuple-element.9) | copy-start | bytes 393220
  5.2 141.2 %all-to-all-start = ((bf16[4,256,2048]{2,1,0:T(8,128)(2,1)}), bf16[4,256,2048]{2,1,0:T(8,128)(2,1)}, u32[]{:S(2)}, u32[]{:S(2)}) async-start(bf16[4,256,2048]{2,1,0:T(8,128)(2,1)} %get-tuple-element.10), calls=%async_computation | async-start | bytes 8388608 | tf_op jit(solution)/shard_map/all_to_all | solution.py:335
  11.7 124.0 %copy-start.5 = (s32[1,8,32]{2,1,0:T(8,128)S(1)}, s32[1,8,32]{2,1,0:T(8,128)}, u32[]{:S(2)}) copy-start(s32[1,8,32]{2,1,0:T(8,128)} %param.11) | copy-start | bytes 3076
  135.7 16.1 %copy-start.1 = (bf16[256,2048]{1,0:T(8,128)(2,1)S(1)}, bf16[256,2048]{1,0:T(8,128)(2,1)}, u32[]{:S(2)}) copy-start(bf16[256,2048]{1,0:T(8,128)(2,1)} %w_ref.1) | copy-start | bytes 3145732
  146.4 11.4 %all-to-all-start.1 = ((bf16[4,128,256]{2,1,0:T(8,128)(2,1)}), bf16[4,128,256]{2,1,0:T(8,128)(2,1)S(1)}, u32[]{:S(2)}, u32[]{:S(2)}) async-start(bf16[4,128,256]{2,1,0:T(8,128)(2,1)} %bitcast.4), calls=%async_computation.1 | async-start | bytes 524288 | tf_op jit(solution)/shard_map/all_to_all | solution.py:335

commit v4 on v3

--- a/solution.py
+++ b/solution.py
@@ -1,3 +1,5 @@
+import functools
+
 import jax
 import jax.numpy as jnp
 from jax import lax
@@ -201,7 +203,8 @@
     def soften(k, bias):
         sums = []
         for r in range(0, rows, chunk):
-            s = s_refs[k][r : r + chunk, :] + bias
+            s = s_refs[k][r : r + chunk, :]
+            s = s if bias is None else s + bias
             first = jnp.where((col < BLOCK) & (col > row + r % BLOCK), -jnp.inf, s[:, :LANES])
             s = jnp.concatenate([first, s[:, LANES:]], axis=1)
             e = jnp.exp(s - jnp.max(s, axis=1, keepdims=True))
@@ -218,17 +221,24 @@
             both = jnp.where(half_lane, pltpu.roll(even, HEAD_DIM, 1), odd)
             out_ref[pl.ds(at, BLOCK), pair * LANES : (pair + 1) * LANES] = both.astype(jnp.bfloat16)
 
-    def step(i, _):
-        first = i * SLOTS
+    def work(first, full):
         biases = [load(0, first)]
         score(0, first)
         for k in range(SLOTS):
             if k + 1 < SLOTS:
                 biases.append(load(k + 1, first + k + 1))
-            sums = soften(k, biases[k])
+            sums = soften(k, None if full else biases[k])
             if k + 1 < SLOTS:
                 score(k + 1, first + k + 1)
             finish(k, first + k, sums)
+
+    def step(i, _):
+        first = i * SLOTS
+        least = sel_ref[first, topk - 1]
+        for k in range(1, SLOTS):
+            least = jnp.minimum(least, sel_ref[first + k, topk - 1])
+        pl.when(least >= 0)(functools.partial(work, first, True))
+        pl.when(least < 0)(functools.partial(work, first, False))
         return 0
 
     lax.fori_loop(0, blocks // SLOTS, step, 0)

time: 161 us -> 162 us (level)
  no operation moved by 1% of the time
where the time goes in v4:
time: 162 us
  blocking collectives  124 us (77%)
  Pallas kernels  20.7 us (13%)
  starting transfers between devices  10.8 us (7%)
  waiting for transfers between devices  4.76 us (3%)
    all_gather x1, blocking collectives, shards(): table = lax.all_gather(codes, 'kv', axis=0, tiled=True)  124 us
    pallas_call x1, Pallas kernels, attend(): pl.pallas_call(attend_body, in_specs=[pl.BlockSpec(memory_space=pltpu.SME...  11.1 us
    all_to_all x2, starting transfers between devices, exchange(): return lax.all_to_all(tiles, 'tp', split_axis=0, concat_axis=0, tiled=True)  10.8 us
    all_to_all x2, waiting for transfers between devices, exchange(): return lax.all_to_all(tiles, 'tp', split_axis=0, concat_axis=0, tiled=True)  4.76 us
    pallas_call x1, Pallas kernels, project_codes(): pl.pallas_call(codes_body, in_specs=[far] * 6, out_specs=[far] * 2, out_s...  4.25 us
  transfers between devices with their start and end apart: 2, of which 1 were waited for; matrix products, arithmetic and copies ran while one was open for 0% of the time, Pallas kernels for 8%

profile of v4, /device:TPU:33, one launch (start us, length us, event | category | flops | bytes accessed | tf_op | source)
XLA Modules:
  0.0 161.5 jit_solution(9134991821305461072)
XLA Ops:
  0.0 0.8 multiply_sine_fusion
  0.9 4.3 %project_codes.1 = (s16[512,128]{1,0:T(8,128)(2,1)}, bf16[4,256,2048]{2,1,0:T(8,128)(2,1)}) custom-call(bf16[512,2048]{1,0:T(8,128)(2,1)} %tok_hbm.1, bf16[64,2048]{1,0:T(8,128)(2,1)} %bitcast.6, bf16[64,2048]{1,0:T(8,128)(2,1)} %bitcast.7, f32[72,128]{1,0:T(8,128)} %get-tuple-element.14.cos_ref.cos_hbm, f32[72,128]{1,0:T(8,128)} %get-tuple-element.13.sin_ref.sin_hbm, ...), custom_call_target="tpu_custom_call" | custom-call | tf_op jit(solution)/shard_map/project_codes/pallas_call | solution.py:119
  5.1 0.0 copy-start
  5.1 0.0 copy-start.2
  5.2 0.0 copy-start.3
  5.2 0.0 copy-start.4
  5.2 0.0 copy-start.6
  5.2 5.4 %all-to-all-start = ((bf16[4,256,2048]{2,1,0:T(8,128)(2,1)}), bf16[4,256,2048]{2,1,0:T(8,128)(2,1)}, u32[]{:S(2)}, u32[]{:S(2)}) async-start(bf16[4,256,2048]{2,1,0:T(8,128)(2,1)} %get-tuple-element.10), calls=%async_computation | async-start | bytes 8388608 | tf_op jit(solution)/shard_map/all_to_all | solution.py:345
  10.6 0.0 copy-done
  10.6 0.0 copy-done.2
  10.6 0.0 copy-done.3
  10.6 0.0 copy-done.4
  10.6 1.1 project_queries.1.q_ref
  11.7 0.0 copy-done.6
  11.7 0.0 copy-start.5
  11.7 124.2 %all-gather.1.table_ref = s16[32768,128]{1,0:T(8,128)(2,1)S(1)} all-gather(s16[512,128]{1,0:T(8,128)(2,1)S(1)} %copy-done.6), channel_id=1, replica_groups=mesh['grp'=2,'kv'=64,'tp'=4] {'kv'}, dimensions={0}, use_global_device_ids=true | all-gather | bytes 8519680 | tf_op jit(solution)/shard_map/all_gather | solution.py:356
  135.9 0.0 copy-done.5
  135.9 11.1 %attend.1.x_ref = bf16[512,256]{1,0:T(8,128)(2,1)} custom-call(s32[8,32]{1,0:T(8,128)S(1)} %bitcast.5, bf16[8,256,128]{2,1,0:T(8,128)(2,1)S(1)} %project_queries.1.q_ref, s16[32768,128]{1,0:T(8,128)(2,1)S(1)} %all-gather.1.table_ref), custom_call_target="tpu_custom_call" | custom-call | tf_op jit(solution)/shard_map/attend/pallas_call | solution.py:253
  147.0 0.0 all-to-all-done.all_hbm
  147.0 5.4 %all-to-all-start.1 = ((bf16[4,128,256]{2,1,0:T(8,128)(2,1)}), bf16[4,128,256]{2,1,0:T(8,128)(2,1)S(1)}, u32[]{:S(2)}, u32[]{:S(2)}) async-start(bf16[4,128,256]{2,1,0:T(8,128)(2,1)} %bitcast.4), calls=%async_computation.1 | async-start | bytes 524288 | tf_op jit(solution)/shard_map/all_to_all | solution.py:345
  152.3 0.0 copy-done.1
  152.3 1.3 keep.1.own_ref
  153.6 4.8 %all-to-all-done.1.x_ref = bf16[4,128,256]{2,1,0:T(8,128)(2,1)S(1)} async-done(((bf16[4,128,256]{2,1,0:T(8,128)(2,1)}), bf16[4,128,256]{2,1,0:T(8,128)(2,1)S(1)}, u32[]{:S(2)}, u32[]{:S(2)}) %all-to-all-start.1) | async-done | bytes 262176 | tf_op jit(solution)/shard_map/all_to_all | solution.py:345
  158.4 3.0 %combine.1 = bf16[128,2048]{1,0:T(8,128)(2,1)} custom-call(s32[1]{0:T(128)} %bitcast.peer_ref, bf16[128,2048]{1,0:T(8,128)(2,1)S(1)} %keep.1.own_ref, bf16[4,128,256]{2,1,0:T(8,128)(2,1)S(1)} %all-to-all-done.1.x_ref, bf16[4,256,2048]{2,1,0:T(8,128)(2,1)} %all-to-all-done.all_hbm), custom_call_target="tpu_custom_call" | custom-call | tf_op jit(solution)/shard_map/combine/pallas_call | solution.py:313
  (3 shorter events, 0.0 us)
Async XLA Ops:
  5.1 5.4 %copy-start = (bf16[512,2048]{1,0:T(8,128)(2,1)S(1)}, bf16[512,2048]{1,0:T(8,128)(2,1)}, u32[]{:S(2)}) copy-start(bf16[512,2048]{1,0:T(8,128)(2,1)} %tok_hbm.1) | copy-start | bytes 6291460
  5.1 5.4 %copy-start.2 = (bf16[2048,256]{1,0:T(8,128)(2,1)S(1)}, bf16[2048,256]{1,0:T(8,128)(2,1)}, u32[]{:S(2)}) copy-start(bf16[2048,256]{1,0:T(8,128)(2,1)} %wq_ref.1) | copy-start | bytes 3145732
  5.2 5.4 %copy-start.3 = (f32[72,128]{1,0:T(8,128)S(1)}, f32[72,128]{1,0:T(8,128)}, u32[]{:S(2)}) copy-start(f32[72,128]{1,0:T(8,128)} %get-tuple-element.13.sin_ref.sin_hbm) | copy-start | bytes 110596
  5.2 5.4 %copy-start.4 = (f32[72,128]{1,0:T(8,128)S(1)}, f32[72,128]{1,0:T(8,128)}, u32[]{:S(2)}) copy-start(f32[72,128]{1,0:T(8,128)} %get-tuple-element.14.cos_ref.cos_hbm) | copy-start | bytes 110596
  5.2 6.5 %copy-start.6 = (s16[512,128]{1,0:T(8,128)(2,1)S(1)}, s16[512,128]{1,0:T(8,128)(2,1)}, u32[]{:S(2)}) copy-start(s16[512,128]{1,0:T(8,128)(2,1)} %get-tuple-element.9) | copy-start | bytes 393220
  5.2 141.8 %all-to-all-start = ((bf16[4,256,2048]{2,1,0:T(8,128)(2,1)}), bf16[4,256,2048]{2,1,0:T(8,128)(2,1)}, u32[]{:S(2)}, u32[]{:S(2)}) async-start(bf16[4,256,2048]{2,1,0:T(8,128)(2,1)} %get-tuple-element.10), calls=%async_computation | async-start | bytes 8388608 | tf_op jit(solution)/shard_map/all_to_all | solution.py:345
  11.7 124.2 %copy-start.5 = (s32[1,8,32]{2,1,0:T(8,128)S(1)}, s32[1,8,32]{2,1,0:T(8,128)}, u32[]{:S(2)}) copy-start(s32[1,8,32]{2,1,0:T(8,128)} %param.11) | copy-start | bytes 3076
  135.9 16.4 %copy-start.1 = (bf16[256,2048]{1,0:T(8,128)(2,1)S(1)}, bf16[256,2048]{1,0:T(8,128)(2,1)}, u32[]{:S(2)}) copy-start(bf16[256,2048]{1,0:T(8,128)(2,1)} %w_ref.1) | copy-start | bytes 3145732
  147.0 11.4 %all-to-all-start.1 = ((bf16[4,128,256]{2,1,0:T(8,128)(2,1)}), bf16[4,128,256]{2,1,0:T(8,128)(2,1)S(1)}, u32[]{:S(2)}, u32[]{:S(2)}) async-start(bf16[4,128,256]{2,1,0:T(8,128)(2,1)} %bitcast.4), calls=%async_computation.1 | async-start | bytes 524288 | tf_op jit(solution)/shard_map/all_to_all | solution.py:345
